TPU v7x, 32 devices: a whole 2x2x4 slice. The times are simulated.
32 devices in a mesh: ep: 8 (over z, core), tp: 4 (over y, x).
Axes of the slice: x: 2, y: 2, z: 4, core: 2. Of those that a mesh axis runs over, the one named last changes fastest.
Arguments:
- tokens: bfloat16 [2048, 2048], P('ep', 'tp'), may hold values from -800 to 800
- norm_gain: bfloat16 [2048], P('tp'), may hold values from 0.099609375 to 1.8984375
- w_gate: bfloat16 [8, 2048, 6144], P('ep', None, 'tp'), may hold values from -0.125 to 0.125
- w_up: bfloat16 [8, 2048, 6144], P('ep', None, 'tp'), may hold values from -0.125 to 0.125
- w_down: bfloat16 [8, 6144, 2048], P('ep', 'tp'), may hold values from -1.2757759 to 1.2757759
- routes: int32 [2048, 2], P('ep'), may hold values from 0 to 7, all different within a row; in each aligned block of 256 rows (0 to 255, 256 to 511, ...) at most 128 rows name the same one
- route_weights: float32 [2048, 2], P('ep'), may hold values from 0.1 to 1
- final_gain: bfloat16 [2048], P('tp'), may hold values from 0.099609375 to 1.8984375
Outputs:
- mixed_out: bfloat16 [2048, 2048], P('ep', 'tp')
Inputs may be any that keep to these rules, and one draw needn't show every extreme that they name: `routes`: A token's 2 experts differ. Among the tokens of one index of ep (aligned blocks of 256 rows), no expert is named by more than 128 tokens, a bound that some block reaches.
All inputs are finite; a program needn't handle non-finite values.
Results may differ from a plain program's by a relative error of at most 0.017.
Values may be sent and summed in bfloat16 or wider, within the bound.
A program may use at most 64 MiB of HBM per device.

v0:
```python
import jax
import jax.numpy as jnp
from jax import lax
from jax.sharding import PartitionSpec as P

EPS = 1e-06


def slot_targets(routes, experts, capacity):
    flat = routes.reshape(-1)
    onehot = (flat[:, None] == jnp.arange(experts, dtype=jnp.int32)[None, :]).astype(jnp.int32)
    before = jnp.cumsum(onehot, axis=0) - onehot
    slot = jnp.sum(before * onehot, axis=1)
    return flat * capacity + slot


def local(tokens, norm_gain, w_gate, w_up, w_down, routes, route_weights, final_gain):
    experts = lax.axis_size("ep")
    tok_rows = tokens.shape[0]
    share = tokens.shape[1]
    width = share * lax.axis_size("tp")
    topk = routes.shape[1]
    capacity = 2 * tok_rows * topk // experts
    wide = tokens.astype(jnp.float32)
    input_squares = lax.psum(jnp.sum(wide * wide, axis=1), "tp")
    scale = lax.rsqrt(input_squares / width + EPS)
    normed = (wide * scale[:, None] * norm_gain.astype(jnp.float32)[None, :]).astype(jnp.bfloat16)
    target = slot_targets(routes, experts, capacity)
    sources = jnp.repeat(jnp.arange(tok_rows, dtype=jnp.int32), topk)
    gate_w = w_gate[0]
    up_w = w_up[0]
    down_w = w_down[0]
    outbox = jnp.zeros((experts * capacity, share), jnp.bfloat16).at[target].set(normed[sources])
    inbox = lax.all_to_all(outbox, "ep", split_axis=0, concat_axis=0, tiled=True)
    piece = lax.all_gather(inbox, "tp", axis=1, tiled=True)
    gate = jnp.dot(piece, gate_w, preferred_element_type=jnp.float32)
    up = jnp.dot(piece, up_w, preferred_element_type=jnp.float32)
    hidden = (jax.nn.silu(gate) * up).astype(jnp.bfloat16)
    sums = lax.psum_scatter(
        lax.dot_general(
            down_w, hidden, (((0,), (1,)), ((), ())), preferred_element_type=jnp.float32
        ).astype(jnp.bfloat16),
        "tp",
        scatter_dimension=0,
        tiled=True,
    )
    returned = lax.all_to_all(sums, "ep", split_axis=1, concat_axis=1, tiled=True)
    picked = jnp.take(returned, target, axis=1).reshape(returned.shape[0], tok_rows, topk)
    combined = jnp.einsum("dtk,tk->td", picked.astype(jnp.float32), route_weights)
    local_squares = jnp.sum(combined * combined, axis=1)
    total_squares = lax.psum(local_squares, "tp")
    final_scale = lax.rsqrt(total_squares / width + EPS)
    return (combined * final_scale[:, None] * final_gain.astype(jnp.float32)[None, :]).astype(
        jnp.bfloat16
    )


def solution(mesh):
    in_specs = (
        P("ep", "tp"),
        P("tp"),
        P("ep", None, "tp"),
        P("ep", None, "tp"),
        P("ep", "tp", None),
        P("ep", None),
        P("ep", None),
        P("tp"),
    )
    out_specs = P("ep", "tp")
    return jax.shard_map(local, mesh=mesh, in_specs=in_specs, out_specs=out_specs, check_vma=False)
```

profile of v0, /device:TPU:0, one launch (start us, length us, event | category | flops | bytes accessed | tf_op | source)
XLA Modules:
  0.0 247.3 jit_solution(9177944375881044333)
XLA Ops:
  6.5 0.8 copy.13
  7.6 0.7 broadcast_multiply_fusion
  8.3 1.1 reduce-window.6
  9.5 0.2 slice_reduce_fusion
  10.0 1.1 fusion.12
  11.1 11.4 %psum.14 = f32[256]{0:T(256)S(1)} all-reduce(f32[256]{0:T(256)S(1)} %fusion.12), channel_id=1, replica_groups=mesh['ep'=8,'tp'=4] {'tp'}, use_global_device_ids=true, to_apply=%region_4.5 | all-reduce | flops 256 | bytes 2048 | tf_op jit(solution)/shard_map/psum | solution.py:25
  22.5 0.7 convert_element_type.35
  23.5 1.1 fusion.14
  24.5 5.0 %scatter_custom_fusion = bf16[1024,512]{1,0:T(8,128)(2,1)S(1)} fusion(s32[512]{0:T(512)S(1)} %bitcast.54, bf16[256,512]{1,0:T(8,128)(2,1)S(1)} %fusion.14, s32[1024]{0:T(1024)S(1)} %pad_clamp_fusion.1, bf16[]{:T(256)} %constant.18.clone.1), kind=kCustom, calls=%fused_computation.22 | custom fusion | bytes 1048578 | tf_op jit(solution)/shard_map/scatter | solution.py:33
  29.6 31.3 %all_to_all.24 = bf16[8,128,512]{2,1,0:T(8,128)(2,1)} all-to-all(bf16[8,128,512]{2,1,0:T(8,128)(2,1)S(1)} %bitcast.50), channel_id=1, replica_groups=mesh['ep'=8,'tp'=4] {'ep'}, dimensions={0} | all-to-all | bytes 2097152 | tf_op jit(solution)/shard_map/all_to_all | solution.py:34
  61.0 0.2 reduce-scatter.2.cloned.1.call-start
  61.2 49.4 %all-gather.2.cloned.1.call-done = bf16[1024,2048]{1,0:T(8,128)(2,1)} async-done(((bf16[1024,512]{1,0:T(8,128)(2,1)}), bf16[1024,2048]{1,0:T(8,128)(2,1)}) %all-gather.2.cloned.1.call-update) | async-done | bytes 4194320 | tf_op jit(solution)/shard_map/all_gather | solution.py:35
  110.6 11.7 %fusion.4 = f32[1024,1536]{1,0:T(8,128)} fusion(bf16[1024,2048]{1,0:T(8,128)(2,1)} %all-gather.2.cloned.1.call-done, bf16[1,2048,1536]{2,1,0:T(8,128)(2,1)} %param.10), kind=kOutput, calls=%fused_computation.7 | convolution fusion | flops 6442450944 | bytes 16777216 | tf_op jit(solution)/shard_map/dot_general | solution.py:36
  122.3 21.0 %convert_bitcast_fusion = bf16[2048,1024]{0,1:T(8,128)(2,1)} fusion(bf16[1,1536,2048]{2,1,0:T(8,128)(2,1)} %param.12, f32[1024,1536]{1,0:T(8,128)} %fusion.4, bf16[1024,2048]{1,0:T(8,128)(2,1)} %all-gather.2.cloned.1.call-done, bf16[1,2048,1536]{2,1,0:T(8,128)(2,1)} %param.11), kind=kOutput, calls=%fused_computation.10 | convolution fusion | flops 12896436224 | bytes 27262976 | tf_op jit(solution)/shard_map/dot_general | solution.py:40
  143.4 52.7 %reduce-scatter.2.cloned.1.call-done = bf16[512,1024]{0,1:T(8,128)(2,1)} async-done(((bf16[2048,1024]{0,1:T(8,128)(2,1)}), bf16[512,1024]{0,1:T(8,128)(2,1)}) %reduce-scatter.2.cloned.1.call-update) | async-done | bytes 1048592 | tf_op jit(solution)/shard_map/reduce_scatter | solution.py:39
  196.1 4.6 %all-to-all-start.1 = ((bf16[512,8,128]{0,2,1:T(8,128)(2,1)}), bf16[512,8,128]{0,2,1:T(8,128)(2,1)S(1)}, u32[]{:S(2)}, u32[]{:S(2)}) async-start(bf16[512,8,128]{0,2,1:T(8,128)(2,1)} %bitcast.52), calls=%async_computation.2 | async-start | bytes 2097152 | tf_op jit(solution)/shard_map/all_to_all | solution.py:47
  201.0 0.2 copy.16
  201.1 0.2 copy.18
  201.4 25.9 %all-to-all-done.1 = bf16[512,8,128]{0,2,1:T(8,128)(2,1)S(1)} async-done(((bf16[512,8,128]{0,2,1:T(8,128)(2,1)}), bf16[512,8,128]{0,2,1:T(8,128)(2,1)S(1)}, u32[]{:S(2)}, u32[]{:S(2)}) %all-to-all-start.1) | async-done | bytes 1048608 | tf_op jit(solution)/shard_map/all_to_all | solution.py:47
  227.3 2.0 gather_fusion
  229.2 0.2 gather.11
  229.5 1.1 fusion.21
  230.6 9.0 %psum.15 = f32[256]{0:T(256)S(1)} all-reduce(f32[256]{0:T(256)S(1)} %fusion.15), channel_id=1, replica_groups=mesh['ep'=8,'tp'=4] {'tp'}, use_global_device_ids=true, to_apply=%region_8.9 | all-reduce | flops 256 | bytes 2048 | tf_op jit(solution)/shard_map/psum | solution.py:51
  239.6 0.8 fusion.17
  (30 shorter events, 1.3 us)
Async XLA Ops:
  6.5 104.1 %all-gather.2.cloned.1.call-start = ((), (), s32[]{:S(2)}) async-start(), calls=%async_computation.3 | async-start | bytes 5242880 | tf_op jit(solution)/shard_map/all_gather | solution.py:35
  61.0 135.1 %reduce-scatter.2.cloned.1.call-start = ((), (), s32[]{:S(2)}) async-start(), calls=%async_computation.4 | async-start | bytes 5242880 | tf_op jit(solution)/shard_map/reduce_scatter | solution.py:39
  143.3 57.6 %copy-start = (s32[256,2]{0,1:T(2,128)S(1)}, s32[256,2]{0,1:T(2,128)}, u32[]{:S(2)}) copy-start(s32[256,2]{0,1:T(2,128)} %param.13) | copy-start | bytes 6148
  143.3 57.8 %copy-start.1 = (f32[256,2]{0,1:T(2,128)S(1)}, f32[256,2]{0,1:T(2,128)}, u32[]{:S(2)}) copy-start(f32[256,2]{0,1:T(2,128)} %param.14) | copy-start | bytes 6148
  143.3 58.0 %copy-start.2 = (bf16[512]{0:T(512)(128)(2,1)S(1)}, bf16[512]{0:T(512)(128)(2,1)}, u32[]{:S(2)}) copy-start(bf16[512]{0:T(512)(128)(2,1)} %param.15) | copy-start | bytes 3076
  196.1 31.2 %all-to-all-start.1 = ((bf16[512,8,128]{0,2,1:T(8,128)(2,1)}), bf16[512,8,128]{0,2,1:T(8,128)(2,1)S(1)}, u32[]{:S(2)}, u32[]{:S(2)}) async-start(bf16[512,8,128]{0,2,1:T(8,128)(2,1)} %bitcast.52), calls=%async_computation.2 | async-start | bytes 2097152 | tf_op jit(solution)/shard_map/all_to_all | solution.py:47
Sparse Core Ops, SparseCore 0:
  61.1 49.4 all-gather.1
  143.5 52.5 reduce-scatter.1
where the time goes:
time: 248 us; the launch traced here: 247 us
  waiting for transfers between devices  128 us (52%)
  blocking collectives  51.7 us (21%)
  matrix products  33.8 us (14%)
  between operations  13.6 us (5%)
  local copies, waits for them, and re-layouts  9.53 us (4%)
  other arithmetic  5.79 us (2%)
  starting transfers between devices  4.83 us (2%)
    reduce_scatter x1, waiting for transfers between devices, local(): lax.psum_scatter(lax.dot_general(down_w, hidden, (((0,), (1,)), ((), ()))...  52.7 us
    all_gather x1, waiting for transfers between devices, local(): piece = lax.all_gather(inbox, 'tp', axis=1, tiled=True)  49.4 us
    all_to_all x1, blocking collectives, local(): lax.all_to_all(outbox, 'ep', split_axis=0, concat_axis=0, tiled=True)  31.3 us
    all_to_all x1, waiting for transfers between devices, local(): lax.all_to_all(sums, 'ep', split_axis=1, concat_axis=1, tiled=True)  25.9 us
    dot_general x1, matrix products, local(): lax.dot_general(down_w, hidden, (((0,), (1,)), ((), ())), preferred_eleme...  21 us
    dot_general x1, matrix products, local(): gate = jnp.dot(piece, gate_w, preferred_element_type=jnp.float32)  11.7 us
    psum x1, blocking collectives, local(): input_squares = lax.psum(jnp.sum(wide * wide, axis=1), 'tp')  11.4 us
    psum x1, blocking collectives, local(): total_squares = lax.psum(local_squares, 'tp')  8.95 us
  transfers between devices with their start and end apart: 3, of which 3 were waited for; matrix products, arithmetic and copies ran while one was open for 0% of the time, Pallas kernels for 0%

commit v1 on v0

--- a/solution.py
+++ b/solution.py
@@ -1,9 +1,21 @@
+import functools
 import jax
 import jax.numpy as jnp
 from jax import lax
 from jax.sharding import PartitionSpec as P
 
 EPS = 1e-06
+
+
+def _turn_streams(page, along_dim, ndim_at):
+    p_next = lax.axis_size("ep")
+    main = jnp.split(page, p_next, axis=along_dim)
+    new = jnp.stack(main, axis=0)
+    tile_out = lax.all_to_all(new, "ep", 0, 0)
+    return jnp.concatenate(tile_out, axis=ndim_at)
+
+
+compute_column_up = functools.partial(_turn_streams, along_dim=1, ndim_at=1)
 
 
 def slot_targets(routes, experts, capacity):
@@ -44,7 +56,7 @@
         scatter_dimension=0,
         tiled=True,
     )
-    returned = lax.all_to_all(sums, "ep", split_axis=1, concat_axis=1, tiled=True)
+    returned = compute_column_up(sums)
     picked = jnp.take(returned, target, axis=1).reshape(returned.shape[0], tok_rows, topk)
     combined = jnp.einsum("dtk,tk->td", picked.astype(jnp.float32), route_weights)
     local_squares = jnp.sum(combined * combined, axis=1)

time: 248 us -> 260 us (1.048)
  local copies, waits for them, and re-layouts: 9.53 us -> 22 us
    unnamed x8 -> x15, local copies, waits for them, and re-layouts: 0.99 us -> 11.9 us
where the time goes in v1:
time: 260 us
  waiting for transfers between devices  128 us (49%)
  blocking collectives  51.7 us (20%)
  matrix products  33.8 us (13%)
  local copies, waits for them, and re-layouts  22 us (8%)
  between operations  13.6 us (5%)
  other arithmetic  5.79 us (2%)
  starting transfers between devices  4.83 us (2%)
    reduce_scatter x1, waiting for transfers between devices, local(): lax.psum_scatter(lax.dot_general(down_w, hidden, (((0,), (1,)), ((), ()))...  52.7 us
    all_gather x1, waiting for transfers between devices, local(): piece = lax.all_gather(inbox, 'tp', axis=1, tiled=True)  49.4 us
    all_to_all x1, blocking collectives, local(): lax.all_to_all(outbox, 'ep', split_axis=0, concat_axis=0, tiled=True)  31.3 us
    all_to_all x1, waiting for transfers between devices, _turn_streams(): tile_out = lax.all_to_all(new, 'ep', 0, 0)  25.9 us
    dot_general x1, matrix products, local(): lax.dot_general(down_w, hidden, (((0,), (1,)), ((), ())), preferred_eleme...  21 us
    unnamed x15, local copies, waits for them, and re-layouts  11.9 us
    dot_general x1, matrix products, local(): gate = jnp.dot(piece, gate_w, preferred_element_type=jnp.float32)  11.7 us
    psum x1, blocking collectives, local(): input_squares = lax.psum(jnp.sum(wide * wide, axis=1), 'tp')  11.4 us
  transfers between devices with their start and end apart: 3, of which 3 were waited for; matrix products, arithmetic and copies ran while one was open for 0% of the time, Pallas kernels for 0%

profile of v1, /device:TPU:0, one launch (start us, length us, event | category | flops | bytes accessed | tf_op | source)
XLA Modules:
  0.0 259.7 jit_solution(5530802697532318886)
XLA Ops:
  8.3 1.1 reduce-window.6
  10.0 1.1 fusion.12
  11.1 11.4 %psum.14 = f32[256]{0:T(256)S(1)} all-reduce(f32[256]{0:T(256)S(1)} %fusion.12), channel_id=1, replica_groups=mesh['ep'=8,'tp'=4] {'tp'}, use_global_device_ids=true, to_apply=%region_4.5 | all-reduce | flops 256 | bytes 2048 | tf_op jit(solution)/shard_map/psum | solution.py:37
  23.5 1.1 fusion.14
  24.5 5.0 %scatter_custom_fusion = bf16[1024,512]{1,0:T(8,128)(2,1)S(1)} fusion(s32[512]{0:T(512)S(1)} %bitcast.86, bf16[256,512]{1,0:T(8,128)(2,1)S(1)} %fusion.14, s32[1024]{0:T(1024)S(1)} %pad_clamp_fusion.1, bf16[]{:T(256)} %constant.18.clone.1), kind=kCustom, calls=%fused_computation.22 | custom fusion | bytes 1048578 | tf_op jit(solution)/shard_map/scatter | solution.py:45
  29.6 31.3 %all_to_all.17 = bf16[8,128,512]{2,1,0:T(8,128)(2,1)} all-to-all(bf16[8,128,512]{2,1,0:T(8,128)(2,1)S(1)} %bitcast.83), channel_id=1, replica_groups=mesh['ep'=8,'tp'=4] {'ep'}, dimensions={0} | all-to-all | bytes 2097152 | tf_op jit(solution)/shard_map/all_to_all | solution.py:46
  61.2 49.4 %all-gather.2.cloned.1.call-done = bf16[1024,2048]{1,0:T(8,128)(2,1)} async-done(((bf16[1024,512]{1,0:T(8,128)(2,1)}), bf16[1024,2048]{1,0:T(8,128)(2,1)}) %all-gather.2.cloned.1.call-update) | async-done | bytes 4194320 | tf_op jit(solution)/shard_map/all_gather | solution.py:47
  110.6 11.7 %fusion.4 = f32[1024,1536]{1,0:T(8,128)} fusion(bf16[1024,2048]{1,0:T(8,128)(2,1)} %all-gather.2.cloned.1.call-done, bf16[1,2048,1536]{2,1,0:T(8,128)(2,1)} %param.10), kind=kOutput, calls=%fused_computation.7 | convolution fusion | flops 6442450944 | bytes 16777216 | tf_op jit(solution)/shard_map/dot_general | solution.py:48
  122.3 21.0 %convert_bitcast_fusion = bf16[2048,1024]{0,1:T(8,128)(2,1)} fusion(bf16[1,1536,2048]{2,1,0:T(8,128)(2,1)} %param.12, f32[1024,1536]{1,0:T(8,128)} %fusion.4, bf16[1024,2048]{1,0:T(8,128)(2,1)} %all-gather.2.cloned.1.call-done, bf16[1,2048,1536]{2,1,0:T(8,128)(2,1)} %param.11), kind=kOutput, calls=%fused_computation.10 | convolution fusion | flops 12896436224 | bytes 27262976 | tf_op jit(solution)/shard_map/dot_general | solution.py:52
  143.4 52.7 %reduce-scatter.2.cloned.1.call-done = bf16[512,1024]{0,1:T(8,128)(2,1)} async-done(((bf16[2048,1024]{0,1:T(8,128)(2,1)}), bf16[512,1024]{0,1:T(8,128)(2,1)}) %reduce-scatter.2.cloned.1.call-update) | async-done | bytes 1048592 | tf_op jit(solution)/shard_map/reduce_scatter | solution.py:51
  196.1 1.6 fusion.30
  197.7 1.6 fusion.29
  199.2 1.6 fusion.28
  200.8 1.6 fusion.27
  202.3 1.6 fusion.26
  203.9 1.6 fusion.25
  205.5 1.6 fusion.24
  207.0 1.6 fusion.23
  208.6 4.6 %all-to-all-start.1 = ((bf16[8,512,128]{1,2,0:T(8,128)(2,1)}), bf16[8,512,128]{1,2,0:T(8,128)(2,1)S(1)}, u32[]{:S(2)}, u32[]{:S(2)}) async-start(bf16[8,512,128]{1,2,0:T(8,128)(2,1)} %fusion.23), calls=%async_computation.2 | async-start | bytes 2097152 | tf_op jit(solution)/shard_map/all_to_all | solution.py:14
  213.8 25.9 %all-to-all-done.1 = bf16[8,512,128]{1,2,0:T(8,128)(2,1)S(1)} async-done(((bf16[8,512,128]{1,2,0:T(8,128)(2,1)}), bf16[8,512,128]{1,2,0:T(8,128)(2,1)S(1)}, u32[]{:S(2)}, u32[]{:S(2)}) %all-to-all-start.1) | async-done | bytes 1048608 | tf_op jit(solution)/shard_map/all_to_all | solution.py:14
  239.8 2.0 gather_fusion
  241.9 1.1 fusion.21
  243.1 9.0 %psum.15 = f32[256]{0:T(256)S(1)} all-reduce(f32[256]{0:T(256)S(1)} %fusion.15), channel_id=1, replica_groups=mesh['ep'=8,'tp'=4] {'tp'}, use_global_device_ids=true, to_apply=%region_8.9 | all-reduce | flops 256 | bytes 2048 | tf_op jit(solution)/shard_map/psum | solution.py:63
  252.1 0.8 fusion.17
  (38 shorter events, 4.5 us)
Async XLA Ops:
  6.5 104.1 %all-gather.2.cloned.1.call-start = ((), (), s32[]{:S(2)}) async-start(), calls=%async_computation.3 | async-start | bytes 5242880 | tf_op jit(solution)/shard_map/all_gather | solution.py:47
  61.0 135.1 %reduce-scatter.2.cloned.1.call-start = ((), (), s32[]{:S(2)}) async-start(), calls=%async_computation.4 | async-start | bytes 5242880 | tf_op jit(solution)/shard_map/reduce_scatter | solution.py:51
  143.3 70.1 %copy-start = (s32[256,2]{0,1:T(2,128)S(1)}, s32[256,2]{0,1:T(2,128)}, u32[]{:S(2)}) copy-start(s32[256,2]{0,1:T(2,128)} %param.13) | copy-start | bytes 6148
  143.3 70.3 %copy-start.1 = (f32[256,2]{0,1:T(2,128)S(1)}, f32[256,2]{0,1:T(2,128)}, u32[]{:S(2)}) copy-start(f32[256,2]{0,1:T(2,128)} %param.14) | copy-start | bytes 6148
  143.3 70.5 %copy-start.2 = (bf16[512]{0:T(512)(128)(2,1)S(1)}, bf16[512]{0:T(512)(128)(2,1)}, u32[]{:S(2)}) copy-start(bf16[512]{0:T(512)(128)(2,1)} %param.15) | copy-start | bytes 3076
  208.6 31.2 %all-to-all-start.1 = ((bf16[8,512,128]{1,2,0:T(8,128)(2,1)}), bf16[8,512,128]{1,2,0:T(8,128)(2,1)S(1)}, u32[]{:S(2)}, u32[]{:S(2)}) async-start(bf16[8,512,128]{1,2,0:T(8,128)(2,1)} %fusion.23), calls=%async_computation.2 | async-start | bytes 2097152 | tf_op jit(solution)/shard_map/all_to_all | solution.py:14
Sparse Core Ops, SparseCore 0:
  61.1 49.4 all-gather.1
  143.5 52.5 reduce-scatter.1
